TPU v7x, 512 devices: a whole 4x4x16 slice. The times are simulated.
512 devices in a mesh: vp: 128 (over z, x, core), dp: 4 (over y).
Axes of the slice: x: 4, y: 4, z: 16, core: 2. Of those that a mesh axis runs over, the one named last changes fastest.
Arguments:
- stream: bfloat16 [1024, 2048], P(('dp', 'vp')), may hold values from -60 to 60
- hidden: bfloat16 [1024, 5632], P('dp', 'vp'), may hold values from -6 to 6
- w_down: bfloat16 [5632, 2048], P(None, 'vp'), may hold values from -0.078125 to 0.078125
- final_gain: float32 [2048], replicated, may hold values from 0.1 to 1.9
- vocab: bfloat16 [2048, 32768], P(None, 'vp'), may hold values from -2 to 200
- vocab_bias: float32 [32768], P('vp'), may hold values from -5 to 5
- targets: int32 [1024], P('dp'), may hold values from 0 to 32767
Outputs:
- losses: float32 [1024], P(('dp', 'vp'))
- grad_input: float32 [1024, 2048], P(('dp', 'vp'))
- grad_vocab: float32 [2048, 32768], P('dp', 'vp')
All inputs are finite; a program needn't handle non-finite values.
Results may differ from a plain program's by a relative error of at most 0.02.
Values may be sent and summed in bfloat16 or wider, within the bound.
No kernel may reach another device: no remote copies, remote signals or barrier semaphores. Data moves between devices by JAX's collectives and lax.ppermute only.
A program may use at most 64 MiB of HBM per device.

v0:
```python
import jax
import jax.numpy as jnp
from jax import lax
from jax.sharding import Mesh
from jax.sharding import PartitionSpec as P

VP = ("vp_0", "vp_1", "vp_2")
DP_VP = ("dp", "vp_0", "vp_1", "vp_2")
norm_eps = 1e-06
zloss_weight = 0.001


def joined_along(pieces, dim):
    pieces = jnp.moveaxis(pieces, 0, dim)
    lengths = pieces.shape
    return pieces.reshape(*lengths[:dim], lengths[dim] * lengths[dim + 1], *lengths[dim + 2 :])


def gather_in_order(array, axes, turns):
    pieces = array[None]
    for k in turns:
        pieces = lax.all_gather(pieces, axes[k], axis=0, tiled=True)
    held = [lax.axis_size(axes[k]) for k in reversed(turns)]
    pieces = pieces.reshape(*held, *array.shape)
    turned = sorted(range(len(turns)), key=lambda place: turns[len(turns) - 1 - place])
    return pieces.transpose(*turned, *range(len(turns), pieces.ndim)).reshape(-1, *array.shape)


def whole_of(array, axes, turns, dim):
    return joined_along(gather_in_order(array, axes, turns), dim)


def collected_together(array, axis):
    leaves = jax.tree.leaves(array)
    turns = sorted(range(len(leaves)), key=lambda k: -leaves[k].size)
    width = (1, *leaves[turns[0]].shape)[-1]
    lines = [
        jnp.pad(leaves[k].reshape(-1), (0, -leaves[k].size % width)).reshape(-1, width)
        for k in turns
    ]
    both, at, found = (lax.all_gather(jnp.concatenate(lines), axis), 0, {})
    for k, line in zip(turns, lines):
        section = both[:, at : at + len(line)].reshape(len(both), -1)
        found[k] = section[:, : leaves[k].size].reshape(-1, *leaves[k].shape)
        at += len(line)
    numbers = iter(range(len(leaves)))
    return jax.tree.map(lambda _: found[next(numbers)], array)


def merged_by_axis(array, axes, combine):
    for axis in axes:
        pieces = collected_together(array, axis)
        array = jax.tree.map(lambda part: part[0], pieces)
        for k in range(1, lax.axis_size(axis)):
            array = combine(array, jax.tree.map(lambda part: part[k], pieces))
    return array


def sent_together(arrays, axis, dim, along):
    ends, at = ([], 0)
    for a in arrays[:-1]:
        at += a.shape[along]
        ends.append(at)
    both = jnp.concatenate(arrays, axis=along)
    return tuple(jnp.split(lax.all_gather(both, axis, axis=dim, tiled=True), ends, axis=along))


def combine_stats(first, second):
    top = jnp.maximum(first[0], second[0])
    total = first[1] * jnp.exp(first[0] - top) + second[1] * jnp.exp(second[0] - top)
    return (top, total, first[2] + second[2])


def body(stream, hidden, w_down, final_gain, vocab, vocab_bias, targets):
    rows_dev = stream.shape[0]
    width = stream.shape[1]
    group = targets.shape[0]
    mine = lax.axis_index(VP)
    w_rows = lax.all_to_all(w_down, VP, split_axis=0, concat_axis=1, tiled=True)
    partial_value = jnp.dot(hidden, w_rows, preferred_element_type=jnp.float32)
    arrived = lax.all_to_all(partial_value[:, None, :], VP, split_axis=0, concat_axis=1, tiled=True)
    proj = jnp.sum(arrived, axis=1)
    normin = (stream.astype(jnp.float32) + proj).astype(jnp.bfloat16)
    values = normin.astype(jnp.float32)
    inv = lax.rsqrt(jnp.mean(values * values, axis=1, keepdims=True) + norm_eps)
    normed_own = (values * inv * final_gain).astype(jnp.bfloat16)
    normed = whole_of(normed_own, VP, (1, 0, 2), 0)
    ncols = vocab.shape[1]
    scores = jnp.dot(normed, vocab, preferred_element_type=jnp.float32) + vocab_bias
    local_top = jnp.max(scores, axis=1)
    local_total = jnp.sum(jnp.exp(scores - local_top[:, None]), axis=1)
    column_ids = lax.broadcasted_iota(jnp.int32, (group, ncols), 1) + mine * ncols
    hit = column_ids == targets[:, None]
    local_target = jnp.sum(jnp.where(hit, scores, 0.0), axis=1)
    top, total, target_score = merged_by_axis(
        (local_top, local_total, local_target), VP, combine_stats
    )
    lse = top + jnp.log(total)
    group_losses = lse - target_score + zloss_weight * lse * lse
    losses = lax.dynamic_slice_in_dim(group_losses, mine * rows_dev, rows_dev)
    probs = jnp.exp(scores - lse[:, None])
    dscore = (probs * (1.0 + 2.0 * zloss_weight * lse)[:, None] - jnp.where(hit, 1.0, 0.0)).astype(
        jnp.bfloat16
    )
    feat_group = width // lax.axis_size("dp")
    feat_start = lax.axis_index("dp") * feat_group
    pieces = sent_together((normed, dscore), "dp", 0, 1)
    rows_slice = lax.dynamic_slice_in_dim(pieces[0], feat_start, feat_group, 1)
    grad_vocab = lax.dot_general(
        rows_slice, pieces[1], (((0,), (0,)), ((), ())), preferred_element_type=jnp.float32
    )
    row_term = lax.dot_general(
        dscore, vocab, (((1,), (1,)), ((), ())), preferred_element_type=jnp.float32
    )
    row_parts = lax.all_to_all(
        row_term[:, None, :].astype(jnp.bfloat16), VP, split_axis=0, concat_axis=1, tiled=True
    ).astype(jnp.float32)
    dnormed = jnp.sum(row_parts, axis=1)
    scaled = dnormed * final_gain
    grad_input = inv * (
        scaled - values * inv * inv * jnp.mean(values * scaled, axis=1, keepdims=True)
    )
    return (losses, grad_input, grad_vocab)


def solution(mesh):
    torus = Mesh(mesh.devices.reshape(16, 4, 2, mesh.shape["dp"]), ("vp_0", "vp_1", "vp_2", "dp"))
    return jax.shard_map(
        body,
        mesh=torus,
        in_specs=(P(DP_VP, None), P("dp", VP), P(None, VP), P(), P(None, VP), P(VP), P("dp")),
        out_specs=(P(DP_VP), P(DP_VP, None), P("dp", VP)),
        check_vma=False,
    )
```

profile of v0, /device:TPU:33, one launch (start us, length us, event | category | flops | bytes accessed | tf_op | source)
XLA Modules:
  0.0 378.1 jit_solution(5065636591865383652)
XLA Ops:
  7.2 2.5 all_to_all.30
  10.1 0.8 reshape.1388
  10.9 38.9 %all_to_all.40 = bf16[128,2,352]{2,1,0:T(2,128)(2,1)S(1)} all-to-all(bf16[128,2,352]{2,1,0:T(2,128)(2,1)S(1)} %reshape.1388), channel_id=1, replica_groups=mesh['vp_0'=16,'vp_1'=4,'vp_2'=2,'dp'=4] {'vp_0','vp_1','vp_2'}, dimensions={0} | all-to-all | bytes 360448 | tf_op jit(solution)/shard_map/all_to_all | solution.py:79
  49.8 0.5 reshape.1389
  50.8 2.2 copy.15
  53.0 105.4 %all_to_all.41 = f32[256,1,2048]{2,1,0:T(1,128)S(1)} all-to-all(f32[256,1,2048]{2,1,0:T(1,128)S(1)} %copy.15), channel_id=1, replica_groups=mesh['vp_0'=16,'vp_1'=4,'vp_2'=2,'dp'=4] {'vp_0','vp_1','vp_2'}, dimensions={0} | all-to-all | bytes 4194304 | tf_op jit(solution)/shard_map/all_to_all | solution.py:81
  158.3 6.8 %reduce.6 = f32[256,2048]{1,0:T(8,128)} reduce(f32[256,1,2048]{2,1,0:T(1,128)S(1)} %all_to_all.41, f32[]{:T(128)} %constant.50), dimensions={1}, to_apply=%all_to_all.34.reduce_sub_computation | reduce | bytes 4194308 | tf_op jit(solution)/shard_map/all_to_all | solution.py:81
  165.2 2.5 all_to_all.35
  167.7 0.7 reduce_sum.54
  168.7 9.1 %all-gather.4 = bf16[4,2,2048]{2,1,0:T(2,128)(2,1)S(1)} all-gather(bf16[1,2,2048]{2,1,0:T(2,128)(2,1)S(1)} %fusion.15), channel_id=2, replica_groups=mesh['vp_0'=16,'vp_1'=4,'vp_2'=2,'dp'=4] {'vp_1'}, dimensions={0}, use_global_device_ids=true | all-gather | bytes 40960 | tf_op jit(solution)/shard_map/all_gather | solution.py:22
  177.7 25.1 %all_gather.31 = bf16[64,2,2048]{2,1,0:T(2,128)(2,1)} all-gather(bf16[4,2,2048]{2,1,0:T(2,128)(2,1)S(1)} %all-gather.4), channel_id=1, replica_groups=mesh['vp_0'=16,'vp_1'=4,'vp_2'=2,'dp'=4] {'vp_0'}, dimensions={0}, use_global_device_ids=true | all-gather | bytes 557056 | tf_op jit(solution)/shard_map/all_gather | solution.py:22
  202.9 24.3 %all-gather.11.cloned.1.call-done = bf16[128,2,2048]{2,1,0:T(2,128)(2,1)} async-done(((bf16[64,2,2048]{2,1,0:T(2,128)(2,1)}), bf16[128,2,2048]{2,1,0:T(2,128)(2,1)}) %all-gather.11.cloned.1.call-update) | async-done | bytes 1048592 | tf_op jit(solution)/shard_map/all_gather | solution.py:22
  227.3 2.4 copy.23
  230.2 0.6 fusion.96
  230.9 22.2 %all-gather.5 = f32[16,3,256]{2,1,0:T(4,128)S(1)} all-gather(f32[1,3,256]{2,1,0:T(4,128)S(1)} %maximum_bitcast_fusion), channel_id=3, replica_groups=mesh['vp_0'=16,'vp_1'=4,'vp_2'=2,'dp'=4] {'vp_0'}, dimensions={0}, use_global_device_ids=true | all-gather | bytes 52224 | tf_op jit(solution)/shard_map/all_gather | solution.py:41
  253.2 9.4 %all-gather.6 = f32[4,3,256]{2,1,0:T(4,128)S(1)} all-gather(f32[1,3,256]{2,1,0:T(4,128)S(1)} %maximum_bitcast_fusion.1), channel_id=4, replica_groups=mesh['vp_0'=16,'vp_1'=4,'vp_2'=2,'dp'=4] {'vp_1'}, dimensions={0}, use_global_device_ids=true | all-gather | bytes 15360 | tf_op jit(solution)/shard_map/all_gather | solution.py:41
  262.7 11.5 %all-gather.7 = f32[2,3,256]{2,1,0:T(4,128)S(1)} all-gather(f32[1,3,256]{2,1,0:T(4,128)S(1)} %maximum_bitcast_fusion.2), channel_id=5, replica_groups=mesh['vp_0'=16,'vp_1'=4,'vp_2'=2,'dp'=4] {'vp_2'}, dimensions={0}, use_global_device_ids=true | all-gather | bytes 9216 | tf_op jit(solution)/shard_map/all_gather | solution.py:41
  274.5 1.1 pad_maximum_fusion
  275.6 0.5 fusion
  276.1 0.5 broadcast.44
  276.6 1.4 reduce.9
  278.0 1.5 reshape.1390
  279.5 14.1 %all-to-all-start.2 = ((bf16[128,2,2048]{2,1,0:T(2,128)(2,1)}), bf16[128,2,2048]{2,1,0:T(2,128)(2,1)}, u32[]{:S(2)}, u32[]{:S(2)}) async-start(bf16[128,2,2048]{2,1,0:T(2,128)(2,1)} %reshape.1390), calls=%async_computation.2 | async-start | bytes 2097152 | tf_op jit(solution)/shard_map/all_to_all | solution.py:115
  293.6 0.6 dynamic_slice.6
  294.2 54.6 %all-to-all-done.2 = bf16[128,2,2048]{2,1,0:T(2,128)(2,1)} async-done(((bf16[128,2,2048]{2,1,0:T(2,128)(2,1)}), bf16[128,2,2048]{2,1,0:T(2,128)(2,1)}, u32[]{:S(2)}, u32[]{:S(2)}) %all-to-all-start.2) | async-done | bytes 1048608 | tf_op jit(solution)/shard_map/all_to_all | solution.py:115
  348.8 6.5 %reshape.1391 = bf16[256,1,2048]{2,1,0:T(2,128)(2,1)S(1)} reshape(bf16[128,2,2048]{2,1,0:T(2,128)(2,1)} %all-to-all-done.2) | data formatting | bytes 2097152
  355.3 7.4 %convert_reduce_fusion = f32[256,2048]{1,0:T(8,128)} fusion(bf16[256,1,2048]{2,1,0:T(2,128)(2,1)S(1)} %reshape.1391), kind=kLoop, calls=%fused_computation.3 | loop fusion | flops 524288 | bytes 3145728 | tf_op jit(solution)/shard_map/convert_element_type | solution.py:117
  362.7 2.5 reshape.1359
  365.2 0.7 reduce_sum.58
  366.0 0.7 fusion.12
  366.7 2.2 slice-done
  368.9 2.3 fusion.1
  (40 shorter events, 2.3 us)
Async XLA Ops:
  7.2 223.0 %copy-start = (bf16[2048,256]{1,0:T(8,128)(2,1)S(1)}, bf16[2048,256]{1,0:T(8,128)(2,1)}, u32[]{:S(2)}) copy-start(bf16[2048,256]{1,0:T(8,128)(2,1)} %param.11) | copy-start | bytes 3145732
  7.2 43.1 %copy-start.2 = (bf16[256,44]{0,1:T(8,128)(2,1)S(1)}, bf16[256,44]{0,1:T(8,128)(2,1)}, u32[]{:S(2)}) copy-start(bf16[256,44]{0,1:T(8,128)(2,1)} %param.8) | copy-start | bytes 67588
  7.2 220.1 %all-gather.11.cloned.1.call-start = ((), (), s32[]{:S(2)}) async-start(), calls=%async_computation.3 | async-start | bytes 1572864 | tf_op jit(solution)/shard_map/all_gather | solution.py:22
  167.7 0.8 copy-start.3
  167.7 0.9 copy-start.1
  202.9 163.8 %all-gather.13.cloned.1.call-start = ((), (), s32[]{:S(2)}) async-start(), calls=%async_computation.4 | async-start | bytes 5898240 | tf_op jit(solution)/shard_map/all_gather | solution.py:65
  227.3 2.9 copy-start.5
  229.7 1.1 copy-start.4
  279.5 69.3 %all-to-all-start.2 = ((bf16[128,2,2048]{2,1,0:T(2,128)(2,1)}), bf16[128,2,2048]{2,1,0:T(2,128)(2,1)}, u32[]{:S(2)}, u32[]{:S(2)}) async-start(bf16[128,2,2048]{2,1,0:T(2,128)(2,1)} %reshape.1390), calls=%async_computation.2 | async-start | bytes 2097152 | tf_op jit(solution)/shard_map/all_to_all | solution.py:115
  366.7 2.2 slice-start
Sparse Core Ops, SparseCore 0:
  203.0 24.2 all-gather.10
  275.7 58.3 all-gather.12
where the time goes:
time: 379 us; the launch traced here: 378 us
  blocking collectives  222 us (59%)
  waiting for transfers between devices  79 us (21%)
  local copies, waits for them, and re-layouts  25.6 us (7%)
  other arithmetic  19.6 us (5%)
  between operations  14.3 us (4%)
  starting transfers between devices  14.1 us (4%)
  matrix products  3.86 us (1%)
    all_to_all x1, blocking collectives, body(): lax.all_to_all(partial_value[:, None, :], VP, split_axis=0, concat_axis=1...  105 us
    all_to_all x1, waiting for transfers between devices, body(): lax.all_to_all(row_term[:, None, :].astype(jnp.bfloat16), VP, split_axis=...  54.6 us
    all_gather x3, blocking collectives, collected_together(): both, at, found = (lax.all_gather(jnp.concatenate(lines), axis), 0, {})  43.1 us
    all_to_all x1, blocking collectives, body(): w_rows = lax.all_to_all(w_down, VP, split_axis=0, concat_axis=1, tiled=True)  38.9 us
    all_gather x2, blocking collectives, gather_in_order(): pieces = lax.all_gather(pieces, axes[k], axis=0, tiled=True)  34.2 us
    all_gather x1, waiting for transfers between devices, gather_in_order(): pieces = lax.all_gather(pieces, axes[k], axis=0, tiled=True)  24.3 us
    all_to_all x1, starting transfers between devices, body(): lax.all_to_all(row_term[:, None, :].astype(jnp.bfloat16), VP, split_axis=...  14.1 us
    unnamed x16, local copies, waits for them, and re-layouts  9.37 us
  transfers between devices with their start and end apart: 3, of which 2 were waited for; matrix products, arithmetic and copies ran while one was open for 6% of the time, Pallas kernels for 0%

commit v1 on v0

--- a/solution.py
+++ b/solution.py
@@ -19,7 +19,9 @@
 def gather_in_order(array, axes, turns):
     pieces = array[None]
     for k in turns:
-        pieces = lax.all_gather(pieces, axes[k], axis=0, tiled=True)
+        pieces = jnp.concatenate(
+            lax.all_to_all(jnp.stack([pieces] * lax.axis_size(axes[k])), axes[k], 0, 0), axis=0
+        )
     held = [lax.axis_size(axes[k]) for k in reversed(turns)]
     pieces = pieces.reshape(*held, *array.shape)
     turned = sorted(range(len(turns)), key=lambda place: turns[len(turns) - 1 - place])

time: 379 us -> 362 us (0.955)
  blocking collectives: 222 us -> 202 us
    all_gather x2 -> x0, blocking collectives: 34.2 us -> none  [gather_in_order(): pieces = lax.all_gather(pieces, axes[k], axis=0, tiled=True)]
    all_to_all x0 -> x1, waiting for transfers between devices: none -> 24.6 us  [gather_in_order(): lax.all_to_all(jnp.stack([pieces] * lax.axis_size(axes[k])), axes[k], 0, 0)]
    all_gather x1 -> x0, waiting for transfers between devices: 24.3 us -> none  [gather_in_order(): pieces = lax.all_gather(pieces, axes[k], axis=0, tiled=True)]
    all_to_all x0 -> x2, blocking collectives: none -> 16.1 us  [gather_in_order(): lax.all_to_all(jnp.stack([pieces] * lax.axis_size(axes[k])), axes[k], 0, 0)]
    all_to_all x0 -> x1, starting transfers between devices: none -> 5.29 us  [gather_in_order(): lax.all_to_all(jnp.stack([pieces] * lax.axis_size(axes[k])), axes[k], 0, 0)]
where the time goes in v1:
time: 362 us
  blocking collectives  202 us (56%)
  waiting for transfers between devices  79.2 us (22%)
  local copies, waits for them, and re-layouts  25.6 us (7%)
  other arithmetic  20.6 us (6%)
  starting transfers between devices  15.6 us (4%)
  between operations  14.3 us (4%)
  matrix products  3.86 us (1%)
    all_to_all x1, blocking collectives, body(): lax.all_to_all(partial_value[:, None, :], VP, split_axis=0, concat_axis=1...  105 us
    all_to_all x1, waiting for transfers between devices, body(): lax.all_to_all(row_term[:, None, :].astype(jnp.bfloat16), VP, split_axis=...  54.6 us
    all_gather x3, blocking collectives, collected_together(): both, at, found = (lax.all_gather(jnp.concatenate(lines), axis), 0, {})  42.1 us
    all_to_all x1, blocking collectives, body(): w_rows = lax.all_to_all(w_down, VP, split_axis=0, concat_axis=1, tiled=True)  38.9 us
    all_to_all x1, waiting for transfers between devices, gather_in_order(): lax.all_to_all(jnp.stack([pieces] * lax.axis_size(axes[k])), axes[k], 0, 0)  24.6 us
    all_to_all x2, blocking collectives, gather_in_order(): lax.all_to_all(jnp.stack([pieces] * lax.axis_size(axes[k])), axes[k], 0, 0)  16.1 us
    all_to_all x1, starting transfers between devices, body(): lax.all_to_all(row_term[:, None, :].astype(jnp.bfloat16), VP, split_axis=...  10.3 us
    unnamed x16, local copies, waits for them, and re-layouts  9.37 us
  transfers between devices with their start and end apart: 3, of which 2 were waited for; matrix products, arithmetic and copies ran while one was open for 6% of the time, Pallas kernels for 0%

profile of v1, /device:TPU:33, one launch (start us, length us, event | category | flops | bytes accessed | tf_op | source)
XLA Modules:
  0.0 361.6 jit_solution(3653035810607998083)
XLA Ops:
  7.2 2.5 all_to_all.39
  10.0 0.8 reshape.1384
  10.9 38.9 %all_to_all.55 = bf16[128,2,352]{2,1,0:T(2,128)(2,1)S(1)} all-to-all(bf16[128,2,352]{2,1,0:T(2,128)(2,1)S(1)} %reshape.1384), channel_id=1, replica_groups=mesh['vp_0'=16,'vp_1'=4,'vp_2'=2,'dp'=4] {'vp_0','vp_1','vp_2'}, dimensions={0} | all-to-all | bytes 360448 | tf_op jit(solution)/shard_map/all_to_all | solution.py:81
  50.8 2.2 copy.14
  52.9 105.4 %all_to_all.56 = f32[256,1,2048]{2,1,0:T(1,128)S(1)} all-to-all(f32[256,1,2048]{2,1,0:T(1,128)S(1)} %copy.14), channel_id=1, replica_groups=mesh['vp_0'=16,'vp_1'=4,'vp_2'=2,'dp'=4] {'vp_0','vp_1','vp_2'}, dimensions={0} | all-to-all | bytes 4194304 | tf_op jit(solution)/shard_map/all_to_all | solution.py:83
  158.3 6.8 %reduce.6 = f32[256,2048]{1,0:T(8,128)} reduce(f32[256,1,2048]{2,1,0:T(1,128)S(1)} %all_to_all.56, f32[]{:T(128)} %constant.50), dimensions={1}, to_apply=%all_to_all.43.reduce_sub_computation | reduce | bytes 4194308 | tf_op jit(solution)/shard_map/all_to_all | solution.py:83
  165.2 2.5 all_to_all.44
  167.7 0.7 reduce_sum.54
  168.7 6.7 %all_to_all.57 = bf16[4,1,2,2048]{3,2,1,0:T(2,128)(2,1)S(1)} all-to-all(bf16[4,1,2,2048]{3,2,1,0:T(2,128)(2,1)S(1)} %stack.9), channel_id=1, replica_groups=mesh['vp_0'=16,'vp_1'=4,'vp_2'=2,'dp'=4] {'vp_1'}, dimensions={0} | all-to-all | bytes 65536 | tf_op jit(solution)/shard_map/all_to_all | solution.py:23
  175.4 1.2 stack.10
  176.6 5.3 %all-to-all-start.3 = ((bf16[16,4,2,2048]{3,2,1,0:T(2,128)(2,1)}), bf16[16,4,2,2048]{3,2,1,0:T(2,128)(2,1)S(1)}, u32[]{:S(2)}, u32[]{:S(2)}) async-start(bf16[16,4,2,2048]{3,2,1,0:T(2,128)(2,1)} %stack.10), calls=%async_computation.3 | async-start | bytes 1048576 | tf_op jit(solution)/shard_map/all_to_all | solution.py:23
  181.9 24.6 %all-to-all-done.3 = bf16[16,4,2,2048]{3,2,1,0:T(2,128)(2,1)S(1)} async-done(((bf16[16,4,2,2048]{3,2,1,0:T(2,128)(2,1)}), bf16[16,4,2,2048]{3,2,1,0:T(2,128)(2,1)S(1)}, u32[]{:S(2)}, u32[]{:S(2)}) %all-to-all-start.3) | async-done | bytes 524320 | tf_op jit(solution)/shard_map/all_to_all | solution.py:23
  206.5 0.9 pad_maximum_fusion.1
  207.5 9.4 %all_to_all.58 = bf16[2,64,2,2048]{3,2,1,0:T(2,128)(2,1)S(1)} all-to-all(bf16[2,64,2,2048]{3,2,1,0:T(2,128)(2,1)S(1)} %pad_maximum_fusion.1), channel_id=1, replica_groups=mesh['vp_0'=16,'vp_1'=4,'vp_2'=2,'dp'=4] {'vp_2'}, dimensions={0} | all-to-all | bytes 2097152 | tf_op jit(solution)/shard_map/all_to_all | solution.py:23
  216.9 1.2 copy.22
  218.6 0.6 fusion.95
  219.3 21.2 %all-gather.3 = f32[16,3,256]{2,1,0:T(4,128)S(1)} all-gather(f32[1,3,256]{2,1,0:T(4,128)S(1)} %maximum_bitcast_fusion), channel_id=2, replica_groups=mesh['vp_0'=16,'vp_1'=4,'vp_2'=2,'dp'=4] {'vp_0'}, dimensions={0}, use_global_device_ids=true | all-gather | bytes 52224 | tf_op jit(solution)/shard_map/all_gather | solution.py:43
  240.6 9.1 %all-gather.4 = f32[4,3,256]{2,1,0:T(4,128)S(1)} all-gather(f32[1,3,256]{2,1,0:T(4,128)S(1)} %maximum_bitcast_fusion.1), channel_id=3, replica_groups=mesh['vp_0'=16,'vp_1'=4,'vp_2'=2,'dp'=4] {'vp_1'}, dimensions={0}, use_global_device_ids=true | all-gather | bytes 15360 | tf_op jit(solution)/shard_map/all_gather | solution.py:43
  249.8 11.8 %all-gather.5 = f32[2,3,256]{2,1,0:T(4,128)S(1)} all-gather(f32[1,3,256]{2,1,0:T(4,128)S(1)} %maximum_bitcast_fusion.2), channel_id=4, replica_groups=mesh['vp_0'=16,'vp_1'=4,'vp_2'=2,'dp'=4] {'vp_2'}, dimensions={0}, use_global_device_ids=true | all-gather | bytes 9216 | tf_op jit(solution)/shard_map/all_gather | solution.py:43
  261.8 1.1 pad_maximum_fusion
  263.9 1.4 reduce.9
  265.3 1.5 reshape.1386
  266.9 10.3 %all-to-all-start.5 = ((bf16[128,2,2048]{2,1,0:T(2,128)(2,1)}), bf16[128,2,2048]{2,1,0:T(2,128)(2,1)}, u32[]{:S(2)}, u32[]{:S(2)}) async-start(bf16[128,2,2048]{2,1,0:T(2,128)(2,1)} %reshape.1386), calls=%async_computation.5 | async-start | bytes 2097152 | tf_op jit(solution)/shard_map/all_to_all | solution.py:117
  277.2 0.6 dynamic_slice.6
  277.8 54.6 %all-to-all-done.5 = bf16[128,2,2048]{2,1,0:T(2,128)(2,1)} async-done(((bf16[128,2,2048]{2,1,0:T(2,128)(2,1)}), bf16[128,2,2048]{2,1,0:T(2,128)(2,1)}, u32[]{:S(2)}, u32[]{:S(2)}) %all-to-all-start.5) | async-done | bytes 1048608 | tf_op jit(solution)/shard_map/all_to_all | solution.py:117
  332.4 6.5 %reshape.1387 = bf16[256,1,2048]{2,1,0:T(2,128)(2,1)S(1)} reshape(bf16[128,2,2048]{2,1,0:T(2,128)(2,1)} %all-to-all-done.5) | data formatting | bytes 2097152
  338.9 7.4 %convert_reduce_fusion = f32[256,2048]{1,0:T(8,128)} fusion(bf16[256,1,2048]{2,1,0:T(2,128)(2,1)S(1)} %reshape.1387), kind=kLoop, calls=%fused_computation.3 | loop fusion | flops 524288 | bytes 3145728 | tf_op jit(solution)/shard_map/convert_element_type | solution.py:119
  346.2 2.5 reshape.1359
  348.7 0.7 reduce_sum.58
  349.6 0.7 fusion.12
  350.3 2.2 slice-done
  352.5 2.3 fusion.1
  (42 shorter events, 3.7 us)
Async XLA Ops:
  7.2 211.4 %copy-start = (bf16[2048,256]{1,0:T(8,128)(2,1)S(1)}, bf16[2048,256]{1,0:T(8,128)(2,1)}, u32[]{:S(2)}) copy-start(bf16[2048,256]{1,0:T(8,128)(2,1)} %param.11) | copy-start | bytes 3145732
  7.2 43.1 %copy-start.2 = (bf16[256,44]{0,1:T(8,128)(2,1)S(1)}, bf16[256,44]{0,1:T(8,128)(2,1)}, u32[]{:S(2)}) copy-start(bf16[256,44]{0,1:T(8,128)(2,1)} %param.8) | copy-start | bytes 67588
  167.7 0.8 copy-start.3
  167.7 0.9 copy-start.1
  176.6 30.0 %all-to-all-start.3 = ((bf16[16,4,2,2048]{3,2,1,0:T(2,128)(2,1)}), bf16[16,4,2,2048]{3,2,1,0:T(2,128)(2,1)S(1)}, u32[]{:S(2)}, u32[]{:S(2)}) async-start(bf16[16,4,2,2048]{3,2,1,0:T(2,128)(2,1)} %stack.10), calls=%async_computation.3 | async-start | bytes 1048576 | tf_op jit(solution)/shard_map/all_to_all | solution.py:23
  181.9 168.4 %all-gather.8.cloned.1.call-start = ((), (), s32[]{:S(2)}) async-start(), calls=%async_computation.6 | async-start | bytes 5898240 | tf_op jit(solution)/shard_map/all_gather | solution.py:67
  216.9 1.6 copy-start.5
  218.1 1.1 copy-start.4
  266.9 65.5 %all-to-all-start.5 = ((bf16[128,2,2048]{2,1,0:T(2,128)(2,1)}), bf16[128,2,2048]{2,1,0:T(2,128)(2,1)}, u32[]{:S(2)}, u32[]{:S(2)}) async-start(bf16[128,2,2048]{2,1,0:T(2,128)(2,1)} %reshape.1386), calls=%async_computation.5 | async-start | bytes 2097152 | tf_op jit(solution)/shard_map/all_to_all | solution.py:117
  350.3 2.2 slice-start
Sparse Core Ops, SparseCore 0:
  263.0 54.7 all-gather.7
